TPU v7x, 512 devices: a whole 4x4x16 slice. The times are simulated.
512 devices in a mesh: gr: 2 (over z_hi), fs: 32 (over z_lo, y), tp: 8 (over x, core).
Axes of the slice: x: 4, y: 4, z: 16 (z_hi: 2, z_lo: 8; z = z_hi * 8 + z_lo), core: 2. Of those that a mesh axis runs over, the one named last changes fastest.
Arguments:
- tokens: bfloat16 [24576, 2048], P(('gr', 'fs')), may hold values from -6 to 6
- route_ids: int32 [24576, 2], P(('gr', 'fs')), may hold values from 0 to 31, as said below
- route_weights: float32 [24576, 2], P(('gr', 'fs')), may hold values from 0.1 to 1
- norm_gain: float32 [2048], P(('gr', 'fs')), may hold values from 0.1 to 1.9
- gate_weight: float32 [32, 2048, 1024], P(None, ('gr', 'fs'), 'tp'), may hold values from -0.125 to 0.125
- up_weight: float32 [32, 2048, 1024], P(None, ('gr', 'fs'), 'tp'), may hold values from -0.125 to 0.125
- down_weight: float32 [32, 1024, 2048], P(None, ('gr', 'fs'), 'tp'), may hold values from -0.1875 to 0.1875
Outputs:
- gate_new: bfloat16 [32, 2048, 1024], P('fs', None, 'tp')
- up_new: bfloat16 [32, 2048, 1024], P('fs', None, 'tp')
- down_new: bfloat16 [32, 1024, 2048], P('fs', 'tp')
- mixed: bfloat16 [24576, 2048], P(('gr', 'fs'), 'tp')
Inputs may be any that keep to these rules, and one draw needn't show every extreme that they name: `route_ids`: each row names two different experts of one group (expert e belongs to group e // 8); in each device's block of 384 rows every expert is named by exactly 24 rows.
All inputs are finite; a program needn't handle non-finite values.
Results may differ from a plain program's by a relative error of at most 0.015.
Values may be sent and summed in bfloat16 or wider, within the bound.
A program may use at most 64 MiB of HBM per device.

v0:
```python
import jax
import jax.numpy as jnp
from jax import lax
from jax.sharding import Mesh
from jax.sharding import PartitionSpec as P

TP = ("tp_0", "tp_1")


def side_by_side(arrays, axis, split_dim, concat_dim, along):
    ends, at = ([], 0)
    for a in arrays[:-1]:
        at += a.shape[along]
        ends.append(at)
    both = jnp.concatenate(arrays, axis=along)
    return tuple(
        jnp.split(
            lax.all_to_all(both, axis, split_axis=split_dim, concat_axis=concat_dim, tiled=True),
            ends,
            axis=along,
        )
    )


def in_one_piece(arrays, axis, dim, along):
    ends, at = ([], 0)
    for a in arrays[:-1]:
        at += a.shape[along]
        ends.append(at)
    both = jnp.concatenate(arrays, axis=along)
    return tuple(jnp.split(lax.all_gather(both, axis, axis=dim, tiled=True), ends, axis=along))


def split_up(array, dim, devices):
    before, after = (array.shape[:dim], array.shape[dim + 1 :])
    return jnp.moveaxis(array.reshape(*before, devices, -1, *after), dim, 0)


def laid_out(pieces, dim):
    pieces = jnp.moveaxis(pieces, 0, dim)
    lengths = pieces.shape
    return pieces.reshape(*lengths[:dim], lengths[dim] * lengths[dim + 1], *lengths[dim + 2 :])


def exchange_in_order(pieces, axes, turns):
    inside = pieces.shape[1:]
    whole = pieces.reshape(*(lax.axis_size(a) for a in axes), *inside)
    for k in turns:
        whole = lax.all_to_all(whole, axes[k], k, k, tiled=True)
    return whole.reshape(-1, *inside)


def exchange_by_axis(array, axes, turns, split_dim, concat_dim):
    pieces = split_up(array, split_dim, lax.axis_size(axes))
    return laid_out(exchange_in_order(pieces, axes, turns), concat_dim)


def local(tokens, route_ids, route_weights, norm_gain, gate_weight, up_weight, down_weight):
    gate_folded = (gate_weight * norm_gain[None, :, None]).astype(jnp.bfloat16)
    up_folded = (up_weight * norm_gain[None, :, None]).astype(jnp.bfloat16)
    down_rounded = down_weight.astype(jnp.bfloat16)
    moved = (
        *side_by_side((gate_folded, up_folded), "fs", 0, 1, 2),
        lax.all_to_all(down_rounded, "fs", split_axis=0, concat_axis=1, tiled=True),
    )
    gate_new, up_new, down_whole = (
        *in_one_piece((moved[0], moved[1]), "gr", 1, 0),
        lax.all_gather(moved[2], "gr", axis=1, tiled=True),
    )
    down_new = exchange_by_axis(down_whole, TP, (1, 0), 1, 2)
    tok = tokens.shape[0]
    width = tokens.shape[1]
    experts = gate_weight.shape[0]
    cap = 2 * tok // experts
    flat_ids = route_ids.reshape(-1)
    onehot = (flat_ids[:, None] == jnp.arange(experts, dtype=jnp.int32)[None, :]).astype(jnp.int32)
    slot = jnp.sum(jnp.cumsum(onehot, axis=0) * onehot, axis=1) - 1
    position = flat_ids * cap + slot
    source = (
        jnp.zeros((experts * cap,), jnp.int32)
        .at[position]
        .set(jnp.arange(2 * tok, dtype=jnp.int32) // 2)
    )
    widened = tokens.astype(jnp.float32)
    normed = (
        widened * lax.rsqrt(jnp.mean(widened * widened, axis=-1, keepdims=True) + 1e-06)
    ).astype(jnp.bfloat16)
    outgoing = normed[source].reshape(experts, cap, width)
    received = lax.all_to_all(outgoing, "fs", split_axis=0, concat_axis=0, tiled=True)
    senders, count, _ = received.shape
    rows = received.reshape(senders * count, width)
    first = jnp.dot(rows, gate_new[0], preferred_element_type=jnp.float32)
    second = jnp.dot(rows, up_new[0], preferred_element_type=jnp.float32)
    hidden = (jax.nn.silu(first) * second).astype(jnp.bfloat16)
    hidden_width = hidden.shape[1]
    down_local = down_whole[0]
    out_columns = down_local.shape[1]
    row_count = hidden.shape[0]
    piece = lax.all_gather(hidden, TP, axis=1, tiled=True)
    piece_width = piece.shape[1]
    blocks = piece_width // hidden_width
    partials = jnp.einsum(
        "mbf,bfd->bmd",
        piece.reshape(row_count, blocks, hidden_width),
        down_local.reshape(blocks, hidden_width, out_columns),
        preferred_element_type=jnp.float32,
    ).astype(jnp.bfloat16)
    total = jnp.sum(partials.astype(jnp.float32), axis=0)
    summed = total.reshape(senders, count, out_columns)
    returned = lax.all_to_all(
        summed.astype(jnp.bfloat16), "fs", split_axis=0, concat_axis=0, tiled=True
    )
    columns = returned.shape[2]
    route_out = returned.reshape(experts * cap, columns)[position].reshape(tok, 2, columns)
    mixed = jnp.sum(route_weights[:, :, None] * route_out.astype(jnp.float32), axis=1).astype(
        jnp.bfloat16
    )
    return (gate_new, up_new, down_new, mixed)


def solution(mesh):
    torus = Mesh(
        mesh.devices.reshape(mesh.shape["gr"], mesh.shape["fs"], 4, 2), ("gr", "fs", "tp_0", "tp_1")
    )
    placed = (
        P(("gr", "fs"), None),
        P(("gr", "fs"), None),
        P(("gr", "fs"), None),
        P(("gr", "fs")),
        P(None, ("gr", "fs"), TP),
        P(None, ("gr", "fs"), TP),
        P(None, ("gr", "fs"), TP),
    )
    return jax.shard_map(
        local,
        mesh=torus,
        in_specs=placed,
        out_specs=(P("fs", None, TP), P("fs", None, TP), P("fs", TP, None), P(("gr", "fs"), TP)),
        check_vma=False,
    )
```

profile of v0, /device:TPU:2, one launch (start us, length us, event | category | flops | bytes accessed | tf_op | source)
XLA Modules:
  0.0 370.6 jit_solution(3223288350482646378)
XLA Ops:
  7.2 1.5 multiply_convert_fusion.1
  8.7 0.9 pad_maximum_fusion
  9.6 15.7 %all-to-all-start = ((bf16[32,32,256]{2,1,0:T(8,128)(2,1)}), bf16[32,32,256]{2,1,0:T(8,128)(2,1)}, u32[]{:S(2)}, u32[]{:S(2)}) async-start(bf16[32,32,256]{2,1,0:T(8,128)(2,1)} %pad_maximum_fusion), calls=%async_computation | async-start | bytes 1048576 | tf_op jit(solution)/shard_map/all_to_all | solution.py:18
  25.7 1.7 reduce-window.6
  27.4 0.3 slice_reduce_fusion
  28.2 3.4 scatter_custom_fusion
  31.6 0.4 fusion
  32.0 0.3 fusion.1
  32.4 4.3 %gather_fusion = bf16[768,2048]{1,0:T(8,128)(2,1)} fusion(bf16[384,2048]{1,0:T(8,128)(2,1)S(1)} %fusion.1, s32[1024]{0:T(1024)S(1)} %pad_clamp_fusion.1), kind=kCustom, calls=%fused_computation | custom fusion | bytes 6294528 | tf_op jit(solution)/shard_map/gather | solution.py:88
  36.6 18.2 %all-to-all-done = bf16[32,32,256]{2,1,0:T(8,128)(2,1)} async-done(((bf16[32,32,256]{2,1,0:T(8,128)(2,1)}), bf16[32,32,256]{2,1,0:T(8,128)(2,1)}, u32[]{:S(2)}, u32[]{:S(2)}) %all-to-all-start) | async-done | bytes 524320 | tf_op jit(solution)/shard_map/all_to_all | solution.py:18
  54.8 6.1 %all-to-all-start.4 = ((bf16[32,24,2048]{2,1,0:T(8,128)(2,1)}), bf16[32,24,2048]{2,1,0:T(8,128)(2,1)S(1)}, u32[]{:S(2)}, u32[]{:S(2)}) async-start(bf16[32,24,2048]{2,1,0:T(8,128)(2,1)} %bitcast.48), calls=%async_computation.4 | async-start | bytes 6291456 | tf_op jit(solution)/shard_map/all_to_all | solution.py:89
  61.0 1.1 fusion.18
  62.1 0.8 pad_maximum_fusion.1
  63.0 66.8 %all-gather.3.cloned.1.call-done = bf16[2,2048,128]{2,1,0:T(8,128)(2,1)} async-done(((bf16[2,1024,128]{2,1,0:T(8,128)(2,1)}), bf16[2,2048,128]{2,1,0:T(8,128)(2,1)}) %all-gather.3.cloned.1.call-update) | async-done | bytes 1048592 | tf_op jit(solution)/shard_map/all_gather | solution.py:31
  129.8 2.2 fusion.17
  132.0 114.4 %all-to-all-done.4 = bf16[32,24,2048]{2,1,0:T(8,128)(2,1)S(1)} async-done(((bf16[32,24,2048]{2,1,0:T(8,128)(2,1)}), bf16[32,24,2048]{2,1,0:T(8,128)(2,1)S(1)}, u32[]{:S(2)}, u32[]{:S(2)}) %all-to-all-start.4) | async-done | bytes 3145760 | tf_op jit(solution)/shard_map/all_to_all | solution.py:89
  246.4 2.1 fusion.6
  248.5 1.7 fusion.4
  250.2 1.1 convert_element_type.42
  251.3 26.3 %all_to_all.44 = bf16[32,16,256]{2,1,0:T(8,128)(2,1)S(1)} all-to-all(bf16[32,16,256]{2,1,0:T(8,128)(2,1)S(1)} %convert_element_type.42), channel_id=1, replica_groups=mesh['gr'=2,'fs'=32,'tp_0'=4,'tp_1'=2] {'fs'}, dimensions={0} | all-to-all | bytes 524288 | tf_op jit(solution)/shard_map/all_to_all | solution.py:64
  277.6 29.7 %all_gather.10 = bf16[1,1024,256]{2,1,0:T(8,128)(2,1)S(1)} all-gather(bf16[1,512,256]{2,1,0:T(8,128)(2,1)S(1)} %bitcast.52), channel_id=1, replica_groups=mesh['gr'=2,'fs'=32,'tp_0'=4,'tp_1'=2] {'gr'}, dimensions={1}, use_global_device_ids=true | all-gather | bytes 786432 | tf_op jit(solution)/shard_map/all_gather | solution.py:68
  307.3 4.2 %all_to_all.45 = bf16[4,2,1,128,256]{4,3,0,2,1:T(8,128)(2,1)S(1)} all-to-all(bf16[4,2,1,128,256]{4,3,0,2,1:T(8,128)(2,1)S(1)} %copy.29), channel_id=1, replica_groups=mesh['gr'=2,'fs'=32,'tp_0'=4,'tp_1'=2] {'tp_1'}, dimensions={1} | all-to-all | bytes 1048576 | tf_op jit(solution)/shard_map/all_to_all | solution.py:49
  311.5 0.8 copy.30
  312.3 5.0 %all-to-all-start.3 = ((bf16[4,2,1,128,256]{4,3,1,2,0:T(8,128)(2,1)}), bf16[4,2,1,128,256]{4,3,1,2,0:T(8,128)(2,1)S(1)}, u32[]{:S(2)}, u32[]{:S(2)}) async-start(bf16[4,2,1,128,256]{4,3,1,2,0:T(8,128)(2,1)} %copy.30), calls=%async_computation.3 | async-start | bytes 1048576 | tf_op jit(solution)/shard_map/all_to_all | solution.py:49
  317.3 3.2 convert_reduce_fusion
  320.5 5.1 %all-to-all-done.3 = bf16[4,2,1,128,256]{4,3,1,2,0:T(8,128)(2,1)S(1)} async-done(((bf16[4,2,1,128,256]{4,3,1,2,0:T(8,128)(2,1)}), bf16[4,2,1,128,256]{4,3,1,2,0:T(8,128)(2,1)S(1)}, u32[]{:S(2)}, u32[]{:S(2)}) %all-to-all-start.3) | async-done | bytes 524320 | tf_op jit(solution)/shard_map/all_to_all | solution.py:49
  325.6 10.0 %all-to-all-start.5 = ((bf16[32,24,256]{2,1,0:T(8,128)(2,1)}), bf16[32,24,256]{2,1,0:T(8,128)(2,1)S(1)}, u32[]{:S(2)}, u32[]{:S(2)}) async-start(bf16[32,24,256]{2,1,0:T(8,128)(2,1)} %bitcast.11), calls=%async_computation.5 | async-start | bytes 786432 | tf_op jit(solution)/shard_map/all_to_all | solution.py:110
  335.7 0.8 copy.39
  336.6 22.4 %all-to-all-done.5 = bf16[32,24,256]{2,1,0:T(8,128)(2,1)S(1)} async-done(((bf16[32,24,256]{2,1,0:T(8,128)(2,1)}), bf16[32,24,256]{2,1,0:T(8,128)(2,1)S(1)}, u32[]{:S(2)}, u32[]{:S(2)}) %all-to-all-start.5) | async-done | bytes 393248 | tf_op jit(solution)/shard_map/all_to_all | solution.py:110
  359.0 2.6 gather_fusion.1
  361.6 0.4 reshape.105
  362.0 1.7 multiply_reduce_fusion
  (31 shorter events, 1.2 us)
Async XLA Ops:
  7.2 18.1 %copy-start.2 = (s32[384,2]{0,1:T(2,128)S(1)}, s32[384,2]{0,1:T(2,128)}, u32[]{:S(2)}) copy-start(s32[384,2]{0,1:T(2,128)} %param.8) | copy-start | bytes 9220
  7.2 24.4 %copy-start = (bf16[384,2048]{1,0:T(8,128)(2,1)S(1)}, bf16[384,2048]{1,0:T(8,128)(2,1)}, u32[]{:S(2)}) copy-start(bf16[384,2048]{1,0:T(8,128)(2,1)} %param.7) | copy-start | bytes 4718596
  9.6 45.3 %all-to-all-start = ((bf16[32,32,256]{2,1,0:T(8,128)(2,1)}), bf16[32,32,256]{2,1,0:T(8,128)(2,1)}, u32[]{:S(2)}, u32[]{:S(2)}) async-start(bf16[32,32,256]{2,1,0:T(8,128)(2,1)} %pad_maximum_fusion), calls=%async_computation | async-start | bytes 1048576 | tf_op jit(solution)/shard_map/all_to_all | solution.py:18
  54.8 191.6 %all-to-all-start.4 = ((bf16[32,24,2048]{2,1,0:T(8,128)(2,1)}), bf16[32,24,2048]{2,1,0:T(8,128)(2,1)S(1)}, u32[]{:S(2)}, u32[]{:S(2)}) async-start(bf16[32,24,2048]{2,1,0:T(8,128)(2,1)} %bitcast.48), calls=%async_computation.4 | async-start | bytes 6291456 | tf_op jit(solution)/shard_map/all_to_all | solution.py:89
  60.9 68.8 %all-gather.3.cloned.1.call-start = ((), (), s32[]{:S(2)}) async-start(), calls=%async_computation.6 | async-start | bytes 1572864 | tf_op jit(solution)/shard_map/all_gather | solution.py:31
  62.9 254.4 %all-gather.5.cloned.1.call-start = ((), (), s32[]{:S(2)}) async-start(), calls=%async_computation.7 | async-start | bytes 1769472 | tf_op jit(solution)/shard_map/all_gather | solution.py:99
  246.4 2.1 copy-start.1
  312.3 23.3 %copy-start.3 = (f32[384,2]{0,1:T(2,128)S(1)}, f32[384,2]{0,1:T(2,128)}, u32[]{:S(2)}) copy-start(f32[384,2]{0,1:T(2,128)} %param.9) | copy-start | bytes 9220
  312.3 13.3 %all-to-all-start.3 = ((bf16[4,2,1,128,256]{4,3,1,2,0:T(8,128)(2,1)}), bf16[4,2,1,128,256]{4,3,1,2,0:T(8,128)(2,1)S(1)}, u32[]{:S(2)}, u32[]{:S(2)}) async-start(bf16[4,2,1,128,256]{4,3,1,2,0:T(8,128)(2,1)} %copy.30), calls=%async_computation.3 | async-start | bytes 1048576 | tf_op jit(solution)/shard_map/all_to_all | solution.py:49
  325.6 33.4 %all-to-all-start.5 = ((bf16[32,24,256]{2,1,0:T(8,128)(2,1)}), bf16[32,24,256]{2,1,0:T(8,128)(2,1)S(1)}, u32[]{:S(2)}, u32[]{:S(2)}) async-start(bf16[32,24,256]{2,1,0:T(8,128)(2,1)} %bitcast.11), calls=%async_computation.5 | async-start | bytes 786432 | tf_op jit(solution)/shard_map/all_to_all | solution.py:110
Sparse Core Ops, SparseCore 0:
  64.4 65.2 all-gather.2
  250.3 28.7 all-gather.4
where the time goes:
time: 371 us
  waiting for transfers between devices  227 us (61%)
  blocking collectives  60.1 us (16%)
  starting transfers between devices  36.8 us (10%)
  local copies, waits for them, and re-layouts  16.8 us (5%)
  between operations  14.3 us (4%)
  other arithmetic  8.64 us (2%)
  matrix products  6.94 us (2%)
    all_to_all x1, waiting for transfers between devices, local(): lax.all_to_all(outgoing, 'fs', split_axis=0, concat_axis=0, tiled=True)  114 us
    all_gather x1, waiting for transfers between devices, in_one_piece(): lax.all_gather(both, axis, axis=dim, tiled=True)  66.8 us
    all_gather x1, blocking collectives, local(): lax.all_gather(moved[2], 'gr', axis=1, tiled=True)  29.7 us
    all_to_all x1, blocking collectives, local(): lax.all_to_all(down_rounded, 'fs', split_axis=0, concat_axis=1, tiled=True)  26.3 us
    all_to_all x1, waiting for transfers between devices, local(): lax.all_to_all(summed.astype(jnp.bfloat16), 'fs', split_axis=0, concat_ax...  22.4 us
    all_to_all x1, waiting for transfers between devices, side_by_side(): lax.all_to_all(both, axis, split_axis=split_dim, concat_axis=concat_dim,...  18.2 us
    all_to_all x1, starting transfers between devices, side_by_side(): lax.all_to_all(both, axis, split_axis=split_dim, concat_axis=concat_dim,...  15.7 us
    all_to_all x1, starting transfers between devices, local(): lax.all_to_all(summed.astype(jnp.bfloat16), 'fs', split_axis=0, concat_ax...  9.96 us
  transfers between devices with their start and end apart: 6, of which 5 were waited for; matrix products, arithmetic and copies ran while one was open for 6% of the time, Pallas kernels for 0%

commit v1 on v0

--- a/solution.py
+++ b/solution.py
@@ -5,6 +5,11 @@
 from jax.sharding import PartitionSpec as P
 
 TP = ("tp_0", "tp_1")
+
+
+def swapped_in(x, name, dim):
+    outgoing = jnp.stack([x] * lax.axis_size(name))
+    return jnp.concatenate(lax.all_to_all(outgoing, name, 0, 0), axis=dim)
 
 
 def side_by_side(arrays, axis, split_dim, concat_dim, along):
@@ -65,7 +70,7 @@
     )
     gate_new, up_new, down_whole = (
         *in_one_piece((moved[0], moved[1]), "gr", 1, 0),
-        lax.all_gather(moved[2], "gr", axis=1, tiled=True),
+        swapped_in(moved[2], "gr", 1),
     )
     down_new = exchange_by_axis(down_whole, TP, (1, 0), 1, 2)
     tok = tokens.shape[0]

time: 371 us -> 376 us (1.013)
  blocking collectives: 60.1 us -> 65.1 us
    all_to_all x0 -> x1, blocking collectives: none -> 34.7 us  [swapped_in(): return jnp.concatenate(lax.all_to_all(outgoing, name, 0, 0), axis=dim)]
    all_gather x1 -> x0, blocking collectives: 29.7 us -> none  [local(): lax.all_gather(moved[2], 'gr', axis=1, tiled=True)]
where the time goes in v1:
time: 376 us; the launch traced here: 375 us
  waiting for transfers between devices  227 us (60%)
  blocking collectives  65.1 us (17%)
  starting transfers between devices  36.2 us (10%)
  local copies, waits for them, and re-layouts  16.8 us (4%)
  between operations  14.3 us (4%)
  other arithmetic  8.68 us (2%)
  matrix products  6.93 us (2%)
    all_to_all x1, waiting for transfers between devices, local(): lax.all_to_all(outgoing, 'fs', split_axis=0, concat_axis=0, tiled=True)  114 us
    all_gather x1, waiting for transfers between devices, in_one_piece(): lax.all_gather(both, axis, axis=dim, tiled=True)  66.8 us
    all_to_all x1, blocking collectives, swapped_in(): return jnp.concatenate(lax.all_to_all(outgoing, name, 0, 0), axis=dim)  34.7 us
    all_to_all x1, blocking collectives, local(): lax.all_to_all(down_rounded, 'fs', split_axis=0, concat_axis=1, tiled=True)  26.3 us
    all_to_all x1, waiting for transfers between devices, local(): lax.all_to_all(summed.astype(jnp.bfloat16), 'fs', split_axis=0, concat_ax...  22.4 us
    all_to_all x1, waiting for transfers between devices, side_by_side(): lax.all_to_all(both, axis, split_axis=split_dim, concat_axis=concat_dim,...  18.2 us
    all_to_all x1, starting transfers between devices, side_by_side(): lax.all_to_all(both, axis, split_axis=split_dim, concat_axis=concat_dim,...  15.7 us
    all_to_all x1, starting transfers between devices, local(): lax.all_to_all(summed.astype(jnp.bfloat16), 'fs', split_axis=0, concat_ax...  9.41 us
  transfers between devices with their start and end apart: 6, of which 5 were waited for; matrix products, arithmetic and copies ran while one was open for 6% of the time, Pallas kernels for 0%

profile of v1, /device:TPU:2, one launch (start us, length us, event | category | flops | bytes accessed | tf_op | source)
XLA Modules:
  0.0 375.1 jit_solution(13393855138463906271)
XLA Ops:
  7.2 1.5 multiply_convert_fusion.1
  8.7 0.9 pad_maximum_fusion
  9.6 15.7 %all-to-all-start = ((bf16[32,32,256]{2,1,0:T(8,128)(2,1)}), bf16[32,32,256]{2,1,0:T(8,128)(2,1)}, u32[]{:S(2)}, u32[]{:S(2)}) async-start(bf16[32,32,256]{2,1,0:T(8,128)(2,1)} %pad_maximum_fusion), calls=%async_computation | async-start | bytes 1048576 | tf_op jit(solution)/shard_map/all_to_all | solution.py:23
  25.7 1.7 reduce-window.6
  27.4 0.3 slice_reduce_fusion
  28.2 3.4 scatter_custom_fusion
  31.6 0.4 fusion
  32.0 0.3 fusion.1
  32.4 4.3 %gather_fusion = bf16[768,2048]{1,0:T(8,128)(2,1)} fusion(bf16[384,2048]{1,0:T(8,128)(2,1)S(1)} %fusion.1, s32[1024]{0:T(1024)S(1)} %pad_clamp_fusion.1), kind=kCustom, calls=%fused_computation | custom fusion | bytes 6294528 | tf_op jit(solution)/shard_map/gather | solution.py:93
  36.6 18.2 %all-to-all-done = bf16[32,32,256]{2,1,0:T(8,128)(2,1)} async-done(((bf16[32,32,256]{2,1,0:T(8,128)(2,1)}), bf16[32,32,256]{2,1,0:T(8,128)(2,1)}, u32[]{:S(2)}, u32[]{:S(2)}) %all-to-all-start) | async-done | bytes 524320 | tf_op jit(solution)/shard_map/all_to_all | solution.py:23
  54.8 6.1 %all-to-all-start.5 = ((bf16[32,24,2048]{2,1,0:T(8,128)(2,1)}), bf16[32,24,2048]{2,1,0:T(8,128)(2,1)S(1)}, u32[]{:S(2)}, u32[]{:S(2)}) async-start(bf16[32,24,2048]{2,1,0:T(8,128)(2,1)} %bitcast.48), calls=%async_computation.5 | async-start | bytes 6291456 | tf_op jit(solution)/shard_map/all_to_all | solution.py:94
  61.0 1.1 fusion.18
  62.1 0.8 pad_maximum_fusion.1
  63.0 66.8 %all-gather.3.cloned.1.call-done = bf16[2,2048,128]{2,1,0:T(8,128)(2,1)} async-done(((bf16[2,1024,128]{2,1,0:T(8,128)(2,1)}), bf16[2,2048,128]{2,1,0:T(8,128)(2,1)}) %all-gather.3.cloned.1.call-update) | async-done | bytes 1048592 | tf_op jit(solution)/shard_map/all_gather | solution.py:36
  129.8 2.2 fusion.17
  132.0 114.4 %all-to-all-done.5 = bf16[32,24,2048]{2,1,0:T(8,128)(2,1)S(1)} async-done(((bf16[32,24,2048]{2,1,0:T(8,128)(2,1)}), bf16[32,24,2048]{2,1,0:T(8,128)(2,1)S(1)}, u32[]{:S(2)}, u32[]{:S(2)}) %all-to-all-start.5) | async-done | bytes 3145760 | tf_op jit(solution)/shard_map/all_to_all | solution.py:94
  246.4 2.1 fusion.6
  248.5 1.7 fusion.4
  250.2 1.1 convert_element_type.42
  251.3 26.3 %all_to_all.46 = bf16[32,16,256]{2,1,0:T(8,128)(2,1)S(1)} all-to-all(bf16[32,16,256]{2,1,0:T(8,128)(2,1)S(1)} %convert_element_type.42), channel_id=1, replica_groups=mesh['gr'=2,'fs'=32,'tp_0'=4,'tp_1'=2] {'fs'}, dimensions={0} | all-to-all | bytes 524288 | tf_op jit(solution)/shard_map/all_to_all | solution.py:69
  277.6 34.7 %all_to_all.47 = bf16[2,1,512,256]{3,2,1,0:T(8,128)(2,1)S(1)} all-to-all(bf16[2,1,512,256]{3,2,1,0:T(8,128)(2,1)S(1)} %pad_maximum_fusion.2), channel_id=1, replica_groups=mesh['gr'=2,'fs'=32,'tp_0'=4,'tp_1'=2] {'gr'}, dimensions={0} | all-to-all | bytes 1048576 | tf_op jit(solution)/shard_map/all_to_all | solution.py:12
  312.4 4.2 %all_to_all.48 = bf16[4,2,1,128,256]{4,3,0,2,1:T(8,128)(2,1)S(1)} all-to-all(bf16[4,2,1,128,256]{4,3,0,2,1:T(8,128)(2,1)S(1)} %copy.25), channel_id=1, replica_groups=mesh['gr'=2,'fs'=32,'tp_0'=4,'tp_1'=2] {'tp_1'}, dimensions={1} | all-to-all | bytes 1048576 | tf_op jit(solution)/shard_map/all_to_all | solution.py:54
  316.5 0.8 copy.26
  317.3 5.0 %all-to-all-start.4 = ((bf16[4,2,1,128,256]{4,3,1,2,0:T(8,128)(2,1)}), bf16[4,2,1,128,256]{4,3,1,2,0:T(8,128)(2,1)S(1)}, u32[]{:S(2)}, u32[]{:S(2)}) async-start(bf16[4,2,1,128,256]{4,3,1,2,0:T(8,128)(2,1)} %copy.26), calls=%async_computation.4 | async-start | bytes 1048576 | tf_op jit(solution)/shard_map/all_to_all | solution.py:54
  322.3 3.2 convert_reduce_fusion
  325.5 5.1 %all-to-all-done.4 = bf16[4,2,1,128,256]{4,3,1,2,0:T(8,128)(2,1)S(1)} async-done(((bf16[4,2,1,128,256]{4,3,1,2,0:T(8,128)(2,1)}), bf16[4,2,1,128,256]{4,3,1,2,0:T(8,128)(2,1)S(1)}, u32[]{:S(2)}, u32[]{:S(2)}) %all-to-all-start.4) | async-done | bytes 524320 | tf_op jit(solution)/shard_map/all_to_all | solution.py:54
  330.6 9.4 %all-to-all-start.6 = ((bf16[32,24,256]{2,1,0:T(8,128)(2,1)}), bf16[32,24,256]{2,1,0:T(8,128)(2,1)S(1)}, u32[]{:S(2)}, u32[]{:S(2)}) async-start(bf16[32,24,256]{2,1,0:T(8,128)(2,1)} %bitcast.11), calls=%async_computation.6 | async-start | bytes 786432 | tf_op jit(solution)/shard_map/all_to_all | solution.py:115
  340.2 0.8 copy.35
  341.1 22.4 %all-to-all-done.6 = bf16[32,24,256]{2,1,0:T(8,128)(2,1)S(1)} async-done(((bf16[32,24,256]{2,1,0:T(8,128)(2,1)}), bf16[32,24,256]{2,1,0:T(8,128)(2,1)S(1)}, u32[]{:S(2)}, u32[]{:S(2)}) %all-to-all-start.6) | async-done | bytes 393248 | tf_op jit(solution)/shard_map/all_to_all | solution.py:115
  363.5 2.6 gather_fusion.1
  366.1 0.4 reshape.106
  366.5 1.7 multiply_reduce_fusion
  (32 shorter events, 1.3 us)
Async XLA Ops:
  7.2 18.1 %copy-start.2 = (s32[384,2]{0,1:T(2,128)S(1)}, s32[384,2]{0,1:T(2,128)}, u32[]{:S(2)}) copy-start(s32[384,2]{0,1:T(2,128)} %param.8) | copy-start | bytes 9220
  7.2 24.4 %copy-start = (bf16[384,2048]{1,0:T(8,128)(2,1)S(1)}, bf16[384,2048]{1,0:T(8,128)(2,1)}, u32[]{:S(2)}) copy-start(bf16[384,2048]{1,0:T(8,128)(2,1)} %param.7) | copy-start | bytes 4718596
  9.6 45.3 %all-to-all-start = ((bf16[32,32,256]{2,1,0:T(8,128)(2,1)}), bf16[32,32,256]{2,1,0:T(8,128)(2,1)}, u32[]{:S(2)}, u32[]{:S(2)}) async-start(bf16[32,32,256]{2,1,0:T(8,128)(2,1)} %pad_maximum_fusion), calls=%async_computation | async-start | bytes 1048576 | tf_op jit(solution)/shard_map/all_to_all | solution.py:23
  54.8 191.6 %all-to-all-start.5 = ((bf16[32,24,2048]{2,1,0:T(8,128)(2,1)}), bf16[32,24,2048]{2,1,0:T(8,128)(2,1)S(1)}, u32[]{:S(2)}, u32[]{:S(2)}) async-start(bf16[32,24,2048]{2,1,0:T(8,128)(2,1)} %bitcast.48), calls=%async_computation.5 | async-start | bytes 6291456 | tf_op jit(solution)/shard_map/all_to_all | solution.py:94
  60.9 68.8 %all-gather.3.cloned.1.call-start = ((), (), s32[]{:S(2)}) async-start(), calls=%async_computation.7 | async-start | bytes 1572864 | tf_op jit(solution)/shard_map/all_gather | solution.py:36
  62.9 259.4 %all-gather.5.cloned.1.call-start = ((), (), s32[]{:S(2)}) async-start(), calls=%async_computation.8 | async-start | bytes 1769472 | tf_op jit(solution)/shard_map/all_gather | solution.py:104
  246.4 2.1 copy-start.1
  317.3 22.7 %copy-start.3 = (f32[384,2]{0,1:T(2,128)S(1)}, f32[384,2]{0,1:T(2,128)}, u32[]{:S(2)}) copy-start(f32[384,2]{0,1:T(2,128)} %param.9) | copy-start | bytes 9220
  317.3 13.3 %all-to-all-start.4 = ((bf16[4,2,1,128,256]{4,3,1,2,0:T(8,128)(2,1)}), bf16[4,2,1,128,256]{4,3,1,2,0:T(8,128)(2,1)S(1)}, u32[]{:S(2)}, u32[]{:S(2)}) async-start(bf16[4,2,1,128,256]{4,3,1,2,0:T(8,128)(2,1)} %copy.26), calls=%async_computation.4 | async-start | bytes 1048576 | tf_op jit(solution)/shard_map/all_to_all | solution.py:54
  330.6 32.8 %all-to-all-start.6 = ((bf16[32,24,256]{2,1,0:T(8,128)(2,1)}), bf16[32,24,256]{2,1,0:T(8,128)(2,1)S(1)}, u32[]{:S(2)}, u32[]{:S(2)}) async-start(bf16[32,24,256]{2,1,0:T(8,128)(2,1)} %bitcast.11), calls=%async_computation.6 | async-start | bytes 786432 | tf_op jit(solution)/shard_map/all_to_all | solution.py:115
Sparse Core Ops, SparseCore 0:
  64.4 65.2 all-gather.2
  250.3 28.7 all-gather.4
